TPU v7x, 32 devices: a whole 2x2x4 slice. The times are simulated.
32 devices in a mesh: grp: 2 (over y), fs: 4 (over z), tp: 4 (over x, core).
Axes of the slice: x: 2, y: 2, z: 4, core: 2. Of those that a mesh axis runs over, the one named last changes fastest.
Arguments:
- tokens: bfloat16 [2048, 2048], P(('grp', 'fs', 'tp')), parts along dimension 0, may hold values from -30 to 30
- gate_master: float32 [2048, 2752], P('fs', 'tp'), may hold values from -0.125 to 0.125
- up_master: float32 [2048, 2752], P('fs', 'tp'), may hold values from -0.125 to 0.125
- down_master: float32 [2048, 2752], P('fs', 'tp'), may hold values from -0.4375 to 0.4375
- norm_gain: float32 [2048], replicated, may hold values from 0.1 to 1.9
- post_gain: float32 [2048], replicated, may hold values from 0.1 to 1.9
- post_bias: float32 [2048], replicated, may hold values from -3 to 3
Outputs:
- gate_ready: bfloat16 [4096, 2752], P('grp', 'tp'), parts along dimension 0
- up_ready: bfloat16 [4096, 2752], P('grp', 'tp'), parts along dimension 0
- down_ready: bfloat16 [4096, 2752], P('grp', 'tp'), parts along dimension 0
- result: bfloat16 [2048, 2048], P(('grp', 'fs', 'tp')), parts along dimension 0
There are 2 independent parts, one for each index of `grp`. A program takes and returns all parts, laid end to end along the dimension named above; an argument that names none is the same for every part. Nothing has to cross between parts.
All inputs are finite; a program needn't handle non-finite values.
Results may differ from a plain program's by a relative error of at most 0.009.
Values may be sent and summed in bfloat16 or wider, within the bound.
A program may use at most 64 MiB of HBM per device.

v0:
```python
import jax
import jax.numpy as jnp
from jax import lax
from jax.sharding import PartitionSpec as P


def finish(wide, branch, post_gain, post_bias):
    mixed = jnp.sqrt(jnp.float32(2.0)) * wide + 0.5 * branch
    center = jnp.mean(mixed, axis=-1, keepdims=True)
    spread = jnp.mean(jnp.square(mixed - center), axis=-1, keepdims=True)
    return ((mixed - center) * lax.rsqrt(spread + 1e-05) * post_gain + post_bias).astype(
        jnp.bfloat16
    )


def local(tokens, gate_master, up_master, down_master, norm_gain, post_gain, post_bias):
    row_count = gate_master.shape[0]
    first_row = lax.axis_index("fs") * row_count
    gain_rows = lax.dynamic_slice_in_dim(norm_gain, first_row, row_count, 0)
    gate_piece = (gain_rows[:, None] * gate_master).astype(jnp.bfloat16)
    up_piece = (gain_rows[:, None] * up_master).astype(jnp.bfloat16)
    down_piece = down_master.astype(jnp.bfloat16)
    gate_ready, up_ready, down_ready = (
        lax.all_gather(gate_piece, "fs", axis=0, tiled=True),
        lax.all_gather(up_piece, "fs", axis=0, tiled=True),
        lax.all_gather(down_piece, "fs", axis=0, tiled=True),
    )
    wide = tokens.astype(jnp.float32)
    normed = (wide * lax.rsqrt(jnp.mean(wide * wide, axis=-1, keepdims=True) + 1e-06)).astype(
        jnp.bfloat16
    )
    piece = lax.all_gather(normed, "tp", axis=0, tiled=True)
    gate = jnp.dot(piece, gate_ready, preferred_element_type=jnp.float32)
    upward = jnp.dot(piece, up_ready, preferred_element_type=jnp.float32)
    hidden = (jax.nn.silu(gate) * upward).astype(jnp.bfloat16)
    branch = lax.psum_scatter(
        lax.dot_general(
            hidden, down_ready, (((1,), (1,)), ((), ())), preferred_element_type=jnp.float32
        ).astype(jnp.bfloat16),
        "tp",
        scatter_dimension=0,
        tiled=True,
    ).astype(jnp.float32)
    result = finish(wide, branch, post_gain, post_bias)
    return (gate_ready, up_ready, down_ready, result)


def solution(mesh):
    return jax.shard_map(
        local,
        mesh=mesh,
        in_specs=(
            P(("grp", "fs", "tp"), None),
            P("fs", "tp"),
            P("fs", "tp"),
            P("fs", "tp"),
            P(),
            P(),
            P(),
        ),
        out_specs=(P("grp", "tp"), P("grp", "tp"), P("grp", "tp"), P(("grp", "fs", "tp"), None)),
        check_vma=False,
    )
```

profile of v0, /device:TPU:0, one launch (start us, length us, event | category | flops | bytes accessed | tf_op | source)
XLA Modules:
  0.0 256.1 jit_solution(3088402425451007015)
XLA Ops:
  7.2 0.0 all-gather.11.cloned.1.call-start
  7.2 1.1 fusion.2
  8.3 1.8 fusion.3
  10.1 0.0 all-gather.11.cloned.1.call-update
  10.1 0.0 all-gather.5.cloned.1.call-start
  10.2 0.8 dynamic_slice.3
  10.9 0.0 copy-start.4
  10.9 3.3 %multiply_convert_fusion = (bf16[512,688]{0,1:T(8,128)(2,1)}, bf16[512,688]{0,1:T(8,128)(2,1)}) fusion(f32[512,688]{0,1:T(8,128)} %param.9, f32[512]{0:T(512)S(1)} %dynamic_slice.3, f32[512,688]{0,1:T(8,128)} %param.8), kind=kLoop, calls=%fused_computation.1 | loop fusion | flops 1409024 | bytes 4229120 | tf_op jit(solution)/shard_map/convert_element_type | solution.py:21
  14.3 0.0 all-gather.5.cloned.1.call-update
  14.3 0.0 all-gather.7.cloned.1.call-start
  14.4 0.7 all-gather.7.cloned.1.call-update
  15.1 0.0 all-gather.9.cloned.1.call-start
  15.1 0.0 copy-done.4
  15.1 0.9 convert_element_type.29
  16.1 0.0 all-gather.9.cloned.1.call-update
  16.1 0.0 reduce-scatter.2.cloned.1.call-start
  16.1 13.6 %all-gather.11.cloned.1.call-done = bf16[256,2048]{1,0:T(8,128)(2,1)} async-done(((bf16[64,2048]{1,0:T(8,128)(2,1)}), bf16[256,2048]{1,0:T(8,128)(2,1)}) %all-gather.11.cloned.1.call-update) | async-done | bytes 1048592 | tf_op jit(solution)/shard_map/all_gather | solution.py:32
  29.7 0.0 copy-start.7
  29.7 60.2 %all-gather.5.cloned.1.call-done = bf16[2048,688]{0,1:T(8,128)(2,1)} async-done(((bf16[512,688]{0,1:T(8,128)(2,1)}), bf16[2048,688]{0,1:T(8,128)(2,1)}) %all-gather.5.cloned.1.call-update) | async-done | bytes 2818064 | tf_op jit(solution)/shard_map/all_gather | solution.py:24
  89.9 3.0 %fusion.7 = f32[256,688]{0,1:T(8,128)S(1)} fusion(bf16[256,2048]{1,0:T(8,128)(2,1)} %all-gather.11.cloned.1.call-done, bf16[2048,688]{0,1:T(8,128)(2,1)} %all-gather.5.cloned.1.call-done), kind=kOutput, calls=%fused_computation.19 | convolution fusion | flops 721420288 | bytes 4571136 | tf_op jit(solution)/shard_map/dot_general | solution.py:33
  93.0 0.0 copy-start
  93.0 0.0 copy-start.5
  93.0 0.0 copy-start.6
  93.0 55.8 %all-gather.7.cloned.1.call-done = bf16[2048,688]{0,1:T(8,128)(2,1)} async-done(((bf16[512,688]{0,1:T(8,128)(2,1)}), bf16[2048,688]{0,1:T(8,128)(2,1)}) %all-gather.7.cloned.1.call-update) | async-done | bytes 2818064 | tf_op jit(solution)/shard_map/all_gather | solution.py:25
  148.8 58.8 %all-gather.9.cloned.1.call-done = bf16[2048,688]{0,1:T(8,128)(2,1)} async-done(((bf16[512,688]{0,1:T(8,128)(2,1)}), bf16[2048,688]{0,1:T(8,128)(2,1)}) %all-gather.9.cloned.1.call-update) | async-done | bytes 2818064 | tf_op jit(solution)/shard_map/all_gather | solution.py:26
  207.6 0.0 copy-done.7
  207.6 6.9 %convolution_convert_fusion = bf16[256,2048]{1,0:T(8,128)(2,1)} fusion(bf16[2048,688]{0,1:T(8,128)(2,1)} %all-gather.9.cloned.1.call-done, bf16[256,2048]{1,0:T(8,128)(2,1)S(1)} %copy-done.7, bf16[2048,688]{0,1:T(8,128)(2,1)} %all-gather.7.cloned.1.call-done, f32[256,688]{0,1:T(8,128)S(1)} %fusion.7), kind=kOutput, calls=%fused_computation | convolution fusion | flops 1444421632 | bytes 8437760 | tf_op jit(solution)/shard_map/dot_general | solution.py:37
  214.5 0.0 copy-start.1
  214.5 0.0 reduce-scatter.2.cloned.1.call-update
  214.5 23.7 %reduce-scatter.2.cloned.1.call-done = bf16[64,2048]{1,0:T(8,128)(2,1)} async-done(((bf16[256,2048]{1,0:T(8,128)(2,1)}), bf16[64,2048]{1,0:T(8,128)(2,1)}) %reduce-scatter.2.cloned.1.call-update) | async-done | bytes 262160 | tf_op jit(solution)/shard_map/reduce_scatter | solution.py:36
  238.2 0.0 copy-done
  238.2 1.2 fusion.5
  239.3 1.2 multiply_reduce_fusion
  240.5 0.0 copy-done.5
  240.6 0.0 copy-done.6
  240.6 1.8 add_convert_fusion
  242.4 0.0 copy-done.1
  242.4 0.0 copy-start.2
  242.4 1.6 copy.14
  244.0 1.3 copy-done.2
  245.2 0.0 copy-start.3
  245.2 1.6 copy.15
  246.8 1.3 copy-done.3
  248.0 1.6 copy.16
  (3 shorter events, 0.0 us)
Async XLA Ops:
  7.2 22.5 %all-gather.11.cloned.1.call-start = ((), (), s32[]{:S(2)}) async-start(), calls=%async_computation.4 | async-start | bytes 1310720 | tf_op jit(solution)/shard_map/all_gather | solution.py:32
  10.1 79.8 %all-gather.5.cloned.1.call-start = ((), (), s32[]{:S(2)}) async-start(), calls=%async_computation.1 | async-start | bytes 3522560 | tf_op jit(solution)/shard_map/all_gather | solution.py:24
  10.9 4.2 %copy-start.4 = (f32[512,688]{0,1:T(8,128)S(1)}, f32[512,688]{0,1:T(8,128)}, u32[]{:S(2)}) copy-start(f32[512,688]{0,1:T(8,128)} %param.10) | copy-start | bytes 4227076
  14.3 134.5 %all-gather.7.cloned.1.call-start = ((), (), s32[]{:S(2)}) async-start(), calls=%async_computation.2 | async-start | bytes 3522560 | tf_op jit(solution)/shard_map/all_gather | solution.py:25
  15.1 192.5 %all-gather.9.cloned.1.call-start = ((), (), s32[]{:S(2)}) async-start(), calls=%async_computation.3 | async-start | bytes 3522560 | tf_op jit(solution)/shard_map/all_gather | solution.py:26
  16.1 222.1 %reduce-scatter.2.cloned.1.call-start = ((), (), s32[]{:S(2)}) async-start(), calls=%async_computation.5 | async-start | bytes 1310720 | tf_op jit(solution)/shard_map/reduce_scatter | solution.py:36
  29.7 177.9 %copy-start.7 = (bf16[256,2048]{1,0:T(8,128)(2,1)S(1)}, bf16[256,2048]{1,0:T(8,128)(2,1)}, u32[]{:S(2)}) copy-start(bf16[256,2048]{1,0:T(8,128)(2,1)} %all-gather.11.cloned.1.call-done) | copy-start | bytes 3145732
  93.0 145.2 %copy-start = (bf16[64,2048]{1,0:T(8,128)(2,1)S(1)}, bf16[64,2048]{1,0:T(8,128)(2,1)}, u32[]{:S(2)}) copy-start(bf16[64,2048]{1,0:T(8,128)(2,1)} %param.7) | copy-start | bytes 786436
  93.0 147.6 %copy-start.5 = (f32[2048]{0:T(1024)S(1)}, f32[2048]{0:T(1024)}, u32[]{:S(2)}) copy-start(f32[2048]{0:T(1024)} %param.13) | copy-start | bytes 24580
  93.0 147.6 %copy-start.6 = (f32[2048]{0:T(1024)S(1)}, f32[2048]{0:T(1024)}, u32[]{:S(2)}) copy-start(f32[2048]{0:T(1024)} %param.12) | copy-start | bytes 24580
  214.5 27.9 %copy-start.1 = (bf16[2048,688]{0,1:T(8,128)(2,1)S(1)}, bf16[2048,688]{0,1:T(8,128)(2,1)}, u32[]{:S(2)}) copy-start(bf16[2048,688]{0,1:T(8,128)(2,1)} %all-gather.5.cloned.1.call-done) | copy-start | bytes 8454148
  242.4 2.8 %copy-start.2 = (bf16[2048,688]{0,1:T(8,128)(2,1)S(1)}, bf16[2048,688]{0,1:T(8,128)(2,1)}, u32[]{:S(2)}) copy-start(bf16[2048,688]{0,1:T(8,128)(2,1)} %all-gather.7.cloned.1.call-done) | copy-start | bytes 8454148
  245.2 2.8 %copy-start.3 = (bf16[2048,688]{0,1:T(8,128)(2,1)S(1)}, bf16[2048,688]{0,1:T(8,128)(2,1)}, u32[]{:S(2)}) copy-start(bf16[2048,688]{0,1:T(8,128)(2,1)} %all-gather.9.cloned.1.call-done) | copy-start | bytes 8454148
Sparse Core Ops, SparseCore 0:
  10.2 19.4 all-gather.10
  31.8 58.0 all-gather.4
  92.1 56.7 all-gather.6
  150.8 56.7 all-gather.8
  214.6 23.4 reduce-scatter.1
where the time goes:
time: 257 us; the launch traced here: 256 us
  waiting for transfers between devices  213 us (83%)
  between operations  13.9 us (5%)
  other arithmetic  11.4 us (4%)
  matrix products  9.93 us (4%)
  local copies, waits for them, and re-layouts  7.97 us (3%)
    all_gather x1, waiting for transfers between devices, local(): lax.all_gather(gate_piece, 'fs', axis=0, tiled=True)  60.2 us
    all_gather x1, waiting for transfers between devices, local(): lax.all_gather(down_piece, 'fs', axis=0, tiled=True)  58.8 us
    all_gather x1, waiting for transfers between devices, local(): lax.all_gather(up_piece, 'fs', axis=0, tiled=True)  55.8 us
    reduce_scatter x1, waiting for transfers between devices, local(): lax.psum_scatter(lax.dot_general(hidden, down_ready, (((1,), (1,)), ((),...  23.7 us
    all_gather x1, waiting for transfers between devices, local(): piece = lax.all_gather(normed, 'tp', axis=0, tiled=True)  13.6 us
    unnamed x19, local copies, waits for them, and re-layouts  7.21 us
    dot_general x1, matrix products, local(): lax.dot_general(hidden, down_ready, (((1,), (1,)), ((), ())), preferred_e...  6.89 us
  transfers between devices with their start and end apart: 5, of which 5 were waited for; matrix products, arithmetic and copies ran while one was open for 3% of the time, Pallas kernels for 0%

commit v1 on v0

--- a/solution.py
+++ b/solution.py
@@ -1,7 +1,14 @@
+import functools
+
 import jax
 import jax.numpy as jnp
 from jax import lax
+from jax.experimental import pallas as pl
+from jax.experimental.pallas import tpu as pltpu
 from jax.sharding import PartitionSpec as P
+
+MESH = pl.DeviceIdType.MESH
+LANES = 128
 
 
 def finish(wide, branch, post_gain, post_bias):
@@ -13,7 +20,7 @@
     )
 
 
-def local(tokens, gate_master, up_master, down_master, norm_gain, post_gain, post_bias):
+def plain(tokens, gate_master, up_master, down_master, norm_gain, post_gain, post_bias):
     row_count = gate_master.shape[0]
     first_row = lax.axis_index("fs") * row_count
     gain_rows = lax.dynamic_slice_in_dim(norm_gain, first_row, row_count, 0)
@@ -45,7 +52,312 @@
     return (gate_ready, up_ready, down_ready, result)
 
 
+def fused_kernel(
+    fs, tp, n, tok_ref, gm_ref, um_ref, dm_ref, gain_ref, pg_ref, pb_ref,
+    go_ref, uo_ref, do_ref, res_ref,
+    wire, fg, fu, fd, toks, hid, parts, got, mixed,
+    up_sem, dn_sem, y_sem, r_sem, ts_sem, tr_sem, ps_sem, pr_sem, o_sem,
+):
+    y, z, t = lax.axis_index("grp"), lax.axis_index("fs"), lax.axis_index("tp")
+    rc, cols = gm_ref.shape
+    r = rc // (2 * n)
+    q, tail = cols // LANES, cols % LANES
+    half = LANES // 2
+    tok_rows, d = tok_ref.shape
+    up_dev = (y, jnp.minimum(z + 1, fs - 1), t)
+    dn_dev = (y, jnp.maximum(z - 1, 0), t)
+    y_dev = (1 - y, z, t)
+    has_up, has_dn = z < fs - 1, z > 0
+    full = (fg, fu, fd)
+    outs = (go_ref, uo_ref, do_ref)
+    masters = (gm_ref, um_ref, dm_ref)
+
+    barrier = pltpu.get_barrier_semaphore()
+
+    def greet(dev):
+        pl.semaphore_signal(barrier, inc=1, device_id=dev, device_id_type=MESH)
+
+    pl.when(has_up)(lambda: greet(up_dev))
+    pl.when(has_dn)(lambda: greet(dn_dev))
+    greet(y_dev)
+    peers = [lax.rem(t + j, tp) for j in range(1, tp)]
+    for peer in peers:
+        greet((y, z, peer))
+
+    def slot(m, b, h, c):
+        return ((m * fs + b) * 2 + h) * n + c
+
+    def hop(s, dev, sem):
+        return pltpu.make_async_remote_copy(
+            src_ref=wire.at[s], dst_ref=wire.at[s], send_sem=sem.at[s], recv_sem=r_sem.at[s],
+            device_id=dev, device_id_type=MESH,
+        )
+
+    def row_of(b, h, c):
+        return pl.multiple_of(b * rc + (h * n + c) * r, r)
+
+    def put_out(m, row, count):
+        pltpu.make_async_copy(
+            full[m].at[pl.ds(row, count)], outs[m].at[pl.ds(row, count)], o_sem.at[m]
+        ).start()
+
+    def rounded(m, h, c):
+        at = pl.ds(pl.multiple_of((h * n + c) * r, r), r)
+        v = masters[m][at, :]
+        if m < 2:
+            v = v * gain_ref[at, :]
+        return v.astype(jnp.bfloat16)
+
+    def pack(m, c):
+        v = rounded(m, y, c)
+        row = row_of(z, y, c)
+        full[m][pl.ds(row, r), :] = v
+        s = slot(m, z, y, c)
+        for k in range(q):
+            wire[s, k * r:(k + 1) * r, :] = v[:, k * LANES:(k + 1) * LANES]
+        if tail:
+            e = v[:, q * LANES:].astype(jnp.float32)
+            gap = jnp.zeros((r // 2, half - tail), jnp.float32)
+            both = [e[:r // 2], gap, e[r // 2:], gap]
+            wire[s, q * r:, :] = jnp.concatenate(both, axis=1).astype(jnp.bfloat16)
+
+    def send_own(m, c):
+        s = slot(m, z, y, c)
+        pl.when(has_up)(lambda: hop(s, up_dev, up_sem).start())
+        pl.when(has_dn)(lambda: hop(s, dn_dev, dn_sem).start())
+
+    def keep_other(m, c):
+        row = row_of(z, 1 - y, c)
+        full[m][pl.ds(row, r), :] = rounded(m, 1 - y, c)
+
+    def unpack(m, b, h, c):
+        s, row = slot(m, b, h, c), row_of(b, h, c)
+        for k in range(q):
+            full[m][pl.ds(row, r), k * LANES:(k + 1) * LANES] = wire[s, k * r:(k + 1) * r, :]
+        if tail:
+            e = wire[s, q * r:, :].astype(jnp.float32)
+            full[m][pl.ds(row, r // 2), q * LANES:] = e[:, :tail].astype(jnp.bfloat16)
+            shifted = pltpu.roll(e, half, 1)
+            at = pl.ds(pl.multiple_of(row + r // 2, r // 2), r // 2)
+            full[m][at, q * LANES:] = shifted[:, :tail].astype(jnp.bfloat16)
+        put_out(m, row, r)
+
+    def down_rows(row):
+        k = row // r
+        w = fd[pl.ds(row, r), :]
+        part = lax.dot_general(
+            hid[...], w, (((1,), (1,)), ((), ())), preferred_element_type=jnp.float32
+        )
+        parts[k] = part.astype(jnp.bfloat16)
+        for j, peer in enumerate(peers):
+            part_copy(k, j, peer).start()
+
+    def part_copy(k, j, peer):
+        return pltpu.make_async_remote_copy(
+            src_ref=parts.at[k, pl.ds(pl.multiple_of(peer * tok_rows, tok_rows), tok_rows)],
+            dst_ref=got.at[t, k],
+            send_sem=ps_sem.at[j, k], recv_sem=pr_sem.at[t, k],
+            device_id=(y, z, peer), device_id_type=MESH,
+        )
+
+    def arrived(m, c, p, after):
+        low, high = z - 1 - p, z + 1 + p
+
+        @pl.when(low >= 0)
+        def _():
+            s = slot(m, low, y, c)
+            hop(s, up_dev, up_sem).wait_recv()
+            pl.when(has_up)(lambda: hop(s, up_dev, up_sem).start())
+            hop(s, y_dev, y_sem).start()
+
+        @pl.when(high <= fs - 1)
+        def _():
+            s = slot(m, high, y, c)
+            hop(s, dn_dev, dn_sem).wait_recv()
+            pl.when(has_dn)(lambda: hop(s, dn_dev, dn_sem).start())
+            hop(s, y_dev, y_sem).start()
+
+        for b, ok in ((low, low >= 0), (high, high <= fs - 1)):
+            @pl.when(ok)
+            def _(b=b):
+                unpack(m, b, y, c)
+                if after:
+                    down_rows(row_of(b, y, c))
+
+    def crossed(m, c, p, after):
+        low, high = z - 1 - p, z + 1 + p
+        for b, ok in ((low, low >= 0), (high, high <= fs - 1)):
+            @pl.when(ok)
+            def _(b=b):
+                hop(slot(m, b, 1 - y, c), y_dev, y_sem).wait_recv()
+                unpack(m, b, 1 - y, c)
+                if after:
+                    down_rows(row_of(b, 1 - y, c))
+
+    first = [(m, c) for c in range(n) for m in (0, 1)]
+    second = [(2, c) for c in range(n)]
+
+    pack(*first[0])
+    wide = tok_ref[...].astype(jnp.float32)
+    scale = lax.rsqrt(jnp.mean(wide * wide, axis=-1, keepdims=True) + 1e-06)
+    toks[t] = (wide * scale).astype(jnp.bfloat16)
+    for pair in first[1:]:
+        pack(*pair)
+    expected = has_up.astype(jnp.int32) + has_dn.astype(jnp.int32) + tp
+    pl.semaphore_wait(barrier, expected)
+    for pair in first:
+        send_own(*pair)
+
+    def tok_copy(j, peer):
+        return pltpu.make_async_remote_copy(
+            src_ref=toks.at[t], dst_ref=toks.at[t],
+            send_sem=ts_sem.at[j], recv_sem=tr_sem.at[t],
+            device_id=(y, z, peer), device_id_type=MESH,
+        )
+
+    for j, peer in enumerate(peers):
+        tok_copy(j, peer).start()
+    for pair in second:
+        pack(*pair)
+    for pair in first + second:
+        keep_other(*pair)
+    for m in range(3):
+        put_out(m, pl.multiple_of(z * rc, rc), rc)
+
+    waiting = []
+    for p in range(fs - 1):
+        for m, c in first:
+            arrived(m, c, p, False)
+            waiting.append((m, c, p))
+            if len(waiting) > 1:
+                crossed(*waiting.pop(0), False)
+    for pair in second:
+        send_own(*pair)
+    ready = False
+    for p in range(fs - 1):
+        for m, c in second:
+            arrived(m, c, p, ready)
+            waiting.append((m, c, p))
+            if len(waiting) > 1:
+                crossed(*waiting.pop(0), ready)
+        if not ready:
+            ready = True
+            while waiting:
+                crossed(*waiting.pop(0), False)
+            for j, peer in enumerate(peers):
+                pltpu.make_async_remote_copy(
+                    src_ref=toks.at[peer], dst_ref=toks.at[peer],
+                    send_sem=ts_sem.at[j], recv_sem=tr_sem.at[peer],
+                    device_id=(y, z, peer), device_id_type=MESH,
+                ).wait_recv()
+            lhs = toks[...].reshape(tp * tok_rows, d)
+            wide_step = 2 * LANES
+            for lo in range(0, cols, wide_step):
+                at = slice(lo, min(lo + wide_step, cols))
+                gate = jnp.dot(lhs, fg[:, at], preferred_element_type=jnp.float32)
+                upward = jnp.dot(lhs, fu[:, at], preferred_element_type=jnp.float32)
+                hid[:, at] = (jax.nn.silu(gate) * upward).astype(jnp.bfloat16)
+            for k in range(2 * n):
+                down_rows(pl.multiple_of(z * rc + k * r, r))
+            for c in range(n):
+                for b, ok in ((z - 1, z - 1 >= 0), (z + 1, z + 1 <= fs - 1)):
+                    @pl.when(ok)
+                    def _(b=b, c=c):
+                        down_rows(row_of(b, 0, c))
+                        down_rows(row_of(b, 1, c))
+    while waiting:
+        crossed(*waiting.pop(0), True)
+
+    chunks = d // r
+    wide = tok_ref[...].astype(jnp.float32)
+    mine = pl.ds(pl.multiple_of(t * tok_rows, tok_rows), tok_rows)
+    for k in range(chunks):
+        branch = parts[k, mine, :].astype(jnp.float32)
+        for j, peer in enumerate(peers):
+            pltpu.make_async_remote_copy(
+                src_ref=got.at[peer, k], dst_ref=got.at[peer, k],
+                send_sem=ps_sem.at[j, k], recv_sem=pr_sem.at[peer, k],
+                device_id=(y, z, peer), device_id_type=MESH,
+            ).wait_recv()
+            branch = branch + got[peer, k].astype(jnp.float32)
+        at = slice(k * r, (k + 1) * r)
+        mixed[:, at] = jnp.sqrt(jnp.float32(2.0)) * wide[:, at] + 0.5 * branch
+    mix = mixed[...]
+    center = jnp.mean(mix, axis=-1, keepdims=True)
+    off = mix - center
+    spread = jnp.mean(jnp.square(off), axis=-1, keepdims=True)
+    res_ref[...] = (
+        off * lax.rsqrt(spread + 1e-05) * pg_ref[...] + pb_ref[...]
+    ).astype(jnp.bfloat16)
+
+    for m in range(3):
+        pltpu.make_async_copy(full[m], outs[m], o_sem.at[m]).wait()
+    for j, peer in enumerate(peers):
+        tok_copy(j, peer).wait_send()
+        for k in range(chunks):
+            part_copy(k, j, peer).wait_send()
+    for m in range(3):
+        for c in range(n):
+            for b in range(fs):
+                s = slot(m, b, y, c)
+                pl.when(has_up & (b <= z))(lambda s=s: hop(s, up_dev, up_sem).wait_send())
+                pl.when(has_dn & (b >= z))(lambda s=s: hop(s, dn_dev, dn_sem).wait_send())
+                pl.when(z != b)(lambda s=s: hop(s, y_dev, y_sem).wait_send())
+
+
+def fused(fs, tp, n, tokens, gate_master, up_master, down_master, norm_gain, post_gain, post_bias):
+    rc, cols = gate_master.shape
+    tok_rows, d = tokens.shape
+    r = rc // (2 * n)
+    q, tail = cols // LANES, cols % LANES
+    slots = 3 * fs * 2 * n
+    first_row = lax.axis_index("fs") * rc
+    gain_rows = lax.dynamic_slice_in_dim(norm_gain, first_row, rc, 0)[:, None]
+    bf = jnp.bfloat16
+    ready = jax.ShapeDtypeStruct((d, cols), bf)
+    vmem = pl.BlockSpec(memory_space=pltpu.VMEM)
+    anywhere = pl.BlockSpec(memory_space=pl.ANY)
+    dma = pltpu.SemaphoreType.DMA
+    return tuple(pl.pallas_call(
+        functools.partial(fused_kernel, fs, tp, n),
+        out_shape=(ready, ready, ready, jax.ShapeDtypeStruct((tok_rows, d), bf)),
+        in_specs=[vmem] * 7,
+        out_specs=(anywhere, anywhere, anywhere, vmem),
+        scratch_shapes=[
+            pltpu.VMEM((slots, q * r + (r // 2 if tail else 0), LANES), bf),
+            pltpu.VMEM((d, cols), bf),
+            pltpu.VMEM((d, cols), bf),
+            pltpu.VMEM((d, cols), bf),
+            pltpu.VMEM((tp, tok_rows, d), bf),
+            pltpu.VMEM((tp * tok_rows, cols), bf),
+            pltpu.VMEM((d // r, tp * tok_rows, r), bf),
+            pltpu.VMEM((tp, d // r, tok_rows, r), bf),
+            pltpu.VMEM((tok_rows, d), jnp.float32),
+            dma((slots,)), dma((slots,)), dma((slots,)), dma((slots,)),
+            dma((tp - 1,)), dma((tp,)),
+            dma((tp - 1, d // r)), dma((tp, d // r)), dma((3,)),
+        ],
+        compiler_params=pltpu.CompilerParams(
+            collective_id=0, has_side_effects=True, vmem_limit_bytes=60 * 2**20
+        ),
+    )(
+        tokens, gate_master, up_master, down_master, gain_rows,
+        post_gain[None, :], post_bias[None, :],
+    ))
+
+
 def solution(mesh):
+    grp, fs, tp = mesh.shape["grp"], mesh.shape["fs"], mesh.shape["tp"]
+
+    def local(tokens, gate_master, *rest):
+        rc, cols = gate_master.shape
+        n = rc // (2 * LANES)
+        fits = grp == 2 and fs > 1 and rc % (2 * LANES) == 0 and 2 * n * fs <= 32
+        fits = fits and cols % LANES <= LANES // 2 and tokens.shape[0] % 16 == 0
+        if fits:
+            return fused(fs, tp, n, tokens, gate_master, *rest)
+        return plain(tokens, gate_master, *rest)
+
     return jax.shard_map(
         local,
         mesh=mesh,

time: 257 us -> 122 us (0.47)
  waiting for transfers between devices: 213 us -> 0 us
  Pallas kernels: 0 us -> 101 us
  between operations: 13.9 us -> 0.66 us
  local copies, waits for them, and re-layouts: 7.97 us -> 20.7 us
  other arithmetic: 11.4 us -> 0 us
  matrix products: 9.93 us -> 0 us
    all_gather x4 -> x0, waiting for transfers between devices: 188 us -> none  [the longest x1 60.2 us: local(): lax.all_gather(gate_piece, 'fs', axis=0, tiled=True)]
    pallas_call x0 -> x1, Pallas kernels: none -> 101 us  [fused(): pl.pallas_call(functools.partial(fused_kernel, fs, tp, n), out_shape=(rea...]
    reduce_scatter x1 -> x0, waiting for transfers between devices: 23.7 us -> none  [local(): lax.psum_scatter(lax.dot_general(hidden, down_ready, (((1,), (1,)), ((),...]
    pallas_call x0 -> x3, local copies, waits for them, and re-layouts: none -> 11.9 us  [fused(): pl.pallas_call(functools.partial(fused_kernel, fs, tp, n), out_shape=(rea...]
    dot_general x2 -> x0, matrix products: 9.93 us -> none  [the longest x1 6.89 us: local(): lax.dot_general(hidden, down_ready, (((1,), (1,)), ((), ())), preferred_e...]
    convert_element_type x4 -> x0, other arithmetic: 7.9 us -> none  [the longest x1 3.34 us: local(): up_piece = (gain_rows[:, None] * up_master).astype(jnp.bfloat16)]
    reduce_sum x3 -> x0, other arithmetic: 3.45 us -> none  [the longest x1 1.19 us: finish(): spread = jnp.mean(jnp.square(mixed - center), axis=-1, keepdims=True)]
    unnamed x19 -> x12, local copies, waits for them, and re-layouts: 7.21 us -> 7.02 us
  transfers between devices with their start and end apart: 5 -> 0, of which waited for: 5 -> 0; matrix products, arithmetic and copies ran while one was open for 3% -> 0% of each run, Pallas kernels for 0% -> 0%
where the time goes in v1:
time: 122 us
  Pallas kernels  101 us (83%)
  local copies, waits for them, and re-layouts  20.7 us (17%)
    pallas_call x1, Pallas kernels, fused(): pl.pallas_call(functools.partial(fused_kernel, fs, tp, n), out_shape=(rea...  101 us
    pallas_call x3, local copies, waits for them, and re-layouts, fused(): pl.pallas_call(functools.partial(fused_kernel, fs, tp, n), out_shape=(rea...  11.9 us
    unnamed x12, local copies, waits for them, and re-layouts  7.02 us

profile of v1, /device:TPU:0, one launch (start us, length us, event | category | flops | bytes accessed | tf_op | source)
XLA Modules:
  0.0 122.0 jit_solution(10746400420537157072)
XLA Ops:
  0.6 0.0 copy-start.1
  0.6 0.9 dynamic_slice.3
  1.5 0.9 copy.20.gain_ref
  2.4 0.0 copy-start.2
  2.4 3.1 %copy.17.gm_ref = f32[512,688]{1,0:T(8,128)} copy(f32[512,688]{0,1:T(8,128)} %param.8) | data formatting | bytes 2818048 | tf_op args[1]
  5.5 0.0 copy-done.1
  5.5 1.6 %copy.18.um_ref = f32[512,688]{1,0:T(8,128)} copy(f32[512,688]{0,1:T(8,128)S(1)} %copy-done.1) | data formatting | bytes 2818048 | tf_op args[2]
  7.1 0.0 copy-done.2
  7.1 1.6 %copy.19.dm_ref = f32[512,688]{1,0:T(8,128)} copy(f32[512,688]{0,1:T(8,128)S(1)} %copy-done.2) | data formatting | bytes 2818048 | tf_op args[3]
  8.7 100.7 %shard_map.102 = (bf16[2048,688]{1,0:T(8,128)(2,1)}, bf16[2048,688]{1,0:T(8,128)(2,1)}, bf16[2048,688]{1,0:T(8,128)(2,1)}, bf16[64,2048]{1,0:T(8,128)(2,1)}) custom-call(bf16[64,2048]{1,0:T(8,128)(2,1)} %tok_ref.1, f32[512,688]{1,0:T(8,128)} %copy.17.gm_ref, f32[512,688]{1,0:T(8,128)} %copy.18.um_ref, f32[512,688]{1,0:T(8,128)} %copy.19.dm_ref, ...), custom_call_target="tpu_custom_call" | custom-call | tf_op jit(solution)/shard_map/pallas_call | solution.py:321
  109.4 4.5 %copy.21 = bf16[2048,688]{0,1:T(8,128)(2,1)} copy(bf16[2048,688]{1,0:T(8,128)(2,1)} %get-tuple-element.8) | data formatting | bytes 5636096 | tf_op jit(solution)/shard_map/pallas_call | solution.py:321
  114.0 0.0 copy-start
  114.0 4.7 %copy.22 = bf16[2048,688]{0,1:T(8,128)(2,1)} copy(bf16[2048,688]{1,0:T(8,128)(2,1)} %get-tuple-element.9) | data formatting | bytes 5636096 | tf_op jit(solution)/shard_map/pallas_call | solution.py:321
  118.7 0.0 copy-done
  118.7 0.0 copy-start.3
  118.7 2.7 %copy.23 = bf16[2048,688]{0,1:T(8,128)(2,1)} copy(bf16[2048,688]{1,0:T(8,128)(2,1)S(1)} %copy-done) | data formatting | bytes 5636096 | tf_op jit(solution)/shard_map/pallas_call | solution.py:321
  121.3 0.0 copy-done.3
  121.3 0.7 copy.25
Async XLA Ops:
  0.6 4.8 %copy-start.1 = (f32[512,688]{0,1:T(8,128)S(1)}, f32[512,688]{0,1:T(8,128)}, u32[]{:S(2)}) copy-start(f32[512,688]{0,1:T(8,128)} %param.9) | copy-start | bytes 4227076
  2.4 4.7 %copy-start.2 = (f32[512,688]{0,1:T(8,128)S(1)}, f32[512,688]{0,1:T(8,128)}, u32[]{:S(2)}) copy-start(f32[512,688]{0,1:T(8,128)} %param.10) | copy-start | bytes 4227076
  114.0 4.7 %copy-start = (bf16[2048,688]{1,0:T(8,128)(2,1)S(1)}, bf16[2048,688]{1,0:T(8,128)(2,1)}, u32[]{:S(2)}) copy-start(bf16[2048,688]{1,0:T(8,128)(2,1)} %get-tuple-element.10) | copy-start | bytes 8454148
  118.7 2.7 %copy-start.3 = (bf16[64,2048]{1,0:T(8,128)(2,1)S(1)}, bf16[64,2048]{1,0:T(8,128)(2,1)}, u32[]{:S(2)}) copy-start(bf16[64,2048]{1,0:T(8,128)(2,1)} %get-tuple-element.19) | copy-start | bytes 786436

commit v2 on v0

--- a/solution.py
+++ b/solution.py
@@ -1,7 +1,14 @@
+import functools
+
 import jax
 import jax.numpy as jnp
 from jax import lax
+from jax.experimental import pallas as pl
+from jax.experimental.pallas import tpu as pltpu
 from jax.sharding import PartitionSpec as P
+
+MESH = pl.DeviceIdType.MESH
+LANES = 128
 
 
 def finish(wide, branch, post_gain, post_bias):
@@ -13,7 +20,7 @@
     )
 
 
-def local(tokens, gate_master, up_master, down_master, norm_gain, post_gain, post_bias):
+def plain(tokens, gate_master, up_master, down_master, norm_gain, post_gain, post_bias):
     row_count = gate_master.shape[0]
     first_row = lax.axis_index("fs") * row_count
     gain_rows = lax.dynamic_slice_in_dim(norm_gain, first_row, row_count, 0)
@@ -45,7 +52,308 @@
     return (gate_ready, up_ready, down_ready, result)
 
 
+def fused_kernel(
+    fs, tp, n, tok_ref, gm_ref, um_ref, dm_ref, gain_ref, pg_ref, pb_ref,
+    go_ref, uo_ref, do_ref, res_ref,
+    stage, fg, fu, fd, toks, acc_g, acc_u, hid, parts, got, mixed,
+    up_sem, dn_sem, y_sem, r_sem, ts_sem, tr_sem, ps_sem, pr_sem, o_sem, i_sem,
+):
+    y, z, t = lax.axis_index("grp"), lax.axis_index("fs"), lax.axis_index("tp")
+    cols, rc = gm_ref.shape
+    tok_rows, d = tok_ref.shape
+    tiles = d // LANES
+    full = (fg, fu, fd)
+    outs = (go_ref, uo_ref, do_ref)
+    masters = (gm_ref, um_ref, dm_ref)
+    up_dev = (y, jnp.minimum(z + 1, fs - 1), t)
+    dn_dev = (y, jnp.maximum(z - 1, 0), t)
+    y_dev = (1 - y, z, t)
+    has_up, has_dn = z < fs - 1, z > 0
+    peers = [lax.rem(t + j, tp) for j in range(1, tp)]
+    first = [(m, c) for m in (0, 1) for c in range(n)]
+    second = [(2, c) for c in range(n)]
+
+    def fetch(m, h, c):
+        k = h * n + c
+        return pltpu.make_async_copy(
+            masters[m].at[:, pl.ds(pl.multiple_of(k * LANES, LANES), LANES)],
+            stage.at[m, k], i_sem.at[m, k],
+        )
+
+    for h in (y, 1 - y):
+        for m, c in first + second:
+            fetch(m, h, c).start()
+
+    barrier = pltpu.get_barrier_semaphore()
+
+    def greet(dev):
+        pl.semaphore_signal(barrier, inc=1, device_id=dev, device_id_type=MESH)
+
+    pl.when(has_up)(lambda: greet(up_dev))
+    pl.when(has_dn)(lambda: greet(dn_dev))
+    greet(y_dev)
+    for peer in peers:
+        greet((y, z, peer))
+
+    def tile_of(b, h, c):
+        return b * (2 * n) + h * n + c
+
+    def hop(m, k, dev, sem):
+        s = m * tiles + k
+        return pltpu.make_async_remote_copy(
+            src_ref=full[m].at[k], dst_ref=full[m].at[k], send_sem=sem.at[s], recv_sem=r_sem.at[s],
+            device_id=dev, device_id_type=MESH,
+        )
+
+    def put_out(m, k):
+        pltpu.make_async_copy(
+            full[m].at[k],
+            outs[m].at[:, pl.ds(pl.multiple_of(k * LANES, LANES), LANES)],
+            o_sem.at[m, k],
+        ).start()
+
+    def keep(m, h, c):
+        fetch(m, h, c).wait()
+        k = tile_of(z, h, c)
+        v = stage[m, h * n + c]
+        if m < 2:
+            v = v * gain_ref[:, pl.ds(pl.multiple_of(k * LANES, LANES), LANES)]
+        full[m][k] = v.astype(jnp.bfloat16)
+
+    def send_own(m, c):
+        k = tile_of(z, y, c)
+        pl.when(has_up)(lambda: hop(m, k, up_dev, up_sem).start())
+        pl.when(has_dn)(lambda: hop(m, k, dn_dev, dn_sem).start())
+
+    def part_copy(k, j, peer):
+        return pltpu.make_async_remote_copy(
+            src_ref=parts.at[k, pl.ds(pl.multiple_of(peer * tok_rows, tok_rows), tok_rows)],
+            dst_ref=got.at[t, k],
+            send_sem=ps_sem.at[j, k], recv_sem=pr_sem.at[t, k],
+            device_id=(y, z, peer), device_id_type=MESH,
+        )
+
+    def down_tile(k):
+        part = jnp.dot(hid[...], fd[k], preferred_element_type=jnp.float32)
+        parts[k] = part.astype(jnp.bfloat16)
+        for j, peer in enumerate(peers):
+            part_copy(k, j, peer).start()
+
+    def add_tiles(m, k, start):
+        acc = (acc_g, acc_u)[m]
+        at = pl.ds(pl.multiple_of(k * LANES, LANES), n * LANES)
+        lhs = toks[:, :, at].reshape(tp * tok_rows, n * LANES)
+        rhs = jnp.concatenate([full[m][k + i] for i in range(n)], axis=1)
+        term = lax.dot_general(
+            lhs, rhs, (((1,), (1,)), ((), ())), preferred_element_type=jnp.float32
+        )
+        acc[...] = term if start else acc[...] + term
+
+    def ends(p):
+        low, high = z - 1 - p, z + 1 + p
+        return ((low, low >= 0), (high, high <= fs - 1))
+
+    sums, downs = [], []
+
+    def later(m, b, ok, h, c):
+        if m == 2:
+            downs.append((ok, lambda: down_tile(tile_of(b, h, c))))
+        elif c == n - 1:
+            sums.append((ok, lambda: add_tiles(m, tile_of(b, h, 0), False)))
+
+    def work(todo, count):
+        for _ in range(min(count, len(todo))):
+            ok, item = todo.pop(0)
+            if ok is None:
+                item()
+            else:
+                pl.when(ok)(item)
+
+    def arrived(m, c, p):
+        (low, has_low), (high, has_high) = ends(p)
+
+        @pl.when(has_low)
+        def _():
+            k = tile_of(low, y, c)
+            hop(m, k, up_dev, up_sem).wait_recv()
+            hop(m, k, y_dev, y_sem).start()
+            pl.when(has_up)(lambda: hop(m, k, up_dev, up_sem).start())
+            put_out(m, k)
+
+        @pl.when(has_high)
+        def _():
+            k = tile_of(high, y, c)
+            hop(m, k, dn_dev, dn_sem).wait_recv()
+            hop(m, k, y_dev, y_sem).start()
+            pl.when(has_dn)(lambda: hop(m, k, dn_dev, dn_sem).start())
+            put_out(m, k)
+
+        for b, ok in ends(p):
+            later(m, b, ok, y, c)
+
+    def crossed(m, c, p):
+        for b, ok in ends(p):
+            @pl.when(ok)
+            def _(b=b):
+                k = tile_of(b, 1 - y, c)
+                hop(m, k, y_dev, y_sem).wait_recv()
+                put_out(m, k)
+            later(m, b, ok, 1 - y, c)
+
+    def tok_copy(j, peer, origin):
+        return pltpu.make_async_remote_copy(
+            src_ref=toks.at[origin], dst_ref=toks.at[origin],
+            send_sem=ts_sem.at[j], recv_sem=tr_sem.at[origin],
+            device_id=(y, z, peer), device_id_type=MESH,
+        )
+
+    wide = tok_ref[...].astype(jnp.float32)
+    scale = lax.rsqrt(jnp.mean(wide * wide, axis=-1, keepdims=True) + 1e-06)
+    toks[t] = (wide * scale).astype(jnp.bfloat16)
+    keep(first[0][0], y, first[0][1])
+    expected = has_up.astype(jnp.int32) + has_dn.astype(jnp.int32) + tp
+    pl.semaphore_wait(barrier, expected)
+    for before, pair in zip(first, first[1:]):
+        keep(pair[0], y, pair[1])
+        send_own(*before)
+    for m, c in second:
+        keep(m, y, c)
+    send_own(*first[-1])
+    for j, peer in enumerate(peers):
+        tok_copy(j, peer, t).start()
+    for m, c in first + second:
+        keep(m, 1 - y, c)
+    for m, c in first + second:
+        for h in range(2):
+            put_out(m, tile_of(z, h, c))
+
+    waiting = []
+    for p in range(fs - 1):
+        for m, c in first:
+            arrived(m, c, p)
+            waiting.append((m, c, p))
+            if len(waiting) > 1:
+                crossed(*waiting.pop(0))
+            if p > 0:
+                work(sums, 4)
+        if p == 0:
+            for j, peer in enumerate(peers):
+                tok_copy(j, peer, peer).wait_recv()
+            own = [
+                (None, lambda m=m, h=h: add_tiles(m, tile_of(z, h, 0), h == 0))
+                for m in (0, 1) for h in (0, 1)
+            ]
+            sums[:0] = own
+    for pair in second:
+        send_own(*pair)
+    for p in range(fs - 1):
+        for m, c in second:
+            arrived(m, c, p)
+            waiting.append((m, c, p))
+            if len(waiting) > 1:
+                crossed(*waiting.pop(0))
+            work(downs if p > 0 else sums, 4)
+        if p == 0:
+            work(sums, len(sums))
+            hid[...] = (jax.nn.silu(acc_g[...]) * acc_u[...]).astype(jnp.bfloat16)
+            downs[:0] = [
+                (None, lambda h=h, c=c: down_tile(tile_of(z, h, c)))
+                for h in (0, 1) for c in range(n)
+            ]
+    while waiting:
+        crossed(*waiting.pop(0))
+    work(downs, len(downs))
+
+    wide = tok_ref[...].astype(jnp.float32)
+    mine = pl.ds(pl.multiple_of(t * tok_rows, tok_rows), tok_rows)
+    for k in range(tiles):
+        branch = parts[k, mine, :].astype(jnp.float32)
+        for j, peer in enumerate(peers):
+            pltpu.make_async_remote_copy(
+                src_ref=got.at[peer, k], dst_ref=got.at[peer, k],
+                send_sem=ps_sem.at[j, k], recv_sem=pr_sem.at[peer, k],
+                device_id=(y, z, peer), device_id_type=MESH,
+            ).wait_recv()
+            branch = branch + got[peer, k].astype(jnp.float32)
+        at = slice(k * LANES, (k + 1) * LANES)
+        mixed[:, at] = jnp.sqrt(jnp.float32(2.0)) * wide[:, at] + 0.5 * branch
+    mix = mixed[...]
+    center = jnp.mean(mix, axis=-1, keepdims=True)
+    off = mix - center
+    spread = jnp.mean(jnp.square(off), axis=-1, keepdims=True)
+    res_ref[...] = (
+        off * lax.rsqrt(spread + 1e-05) * pg_ref[...] + pb_ref[...]
+    ).astype(jnp.bfloat16)
+
+    for j, peer in enumerate(peers):
+        tok_copy(j, peer, t).wait_send()
+        for k in range(tiles):
+            part_copy(k, j, peer).wait_send()
+    for m in range(3):
+        for k in range(tiles):
+            pltpu.make_async_copy(
+                full[m].at[k], outs[m].at[:, k * LANES:(k + 1) * LANES], o_sem.at[m, k]
+            ).wait()
+        for c in range(n):
+            for b in range(fs):
+                k = tile_of(b, y, c)
+                pl.when(has_up & (b <= z))(lambda k=k: hop(m, k, up_dev, up_sem).wait_send())
+                pl.when(has_dn & (b >= z))(lambda k=k: hop(m, k, dn_dev, dn_sem).wait_send())
+                pl.when(z != b)(lambda k=k: hop(m, k, y_dev, y_sem).wait_send())
+
+
+def fused(fs, tp, n, tokens, gate_master, up_master, down_master, norm_gain, post_gain, post_bias):
+    rc, cols = gate_master.shape
+    tok_rows, d = tokens.shape
+    tiles, rows = d // LANES, tp * tok_rows
+    bf, f32 = jnp.bfloat16, jnp.float32
+    ready = jax.ShapeDtypeStruct((cols, d), bf)
+    vmem = pl.BlockSpec(memory_space=pltpu.VMEM)
+    anywhere = pl.BlockSpec(memory_space=pl.ANY)
+    dma = pltpu.SemaphoreType.DMA
+    gate, up, down, result = pl.pallas_call(
+        functools.partial(fused_kernel, fs, tp, n),
+        out_shape=(ready, ready, ready, jax.ShapeDtypeStruct((tok_rows, d), bf)),
+        in_specs=[vmem] + [anywhere] * 3 + [vmem] * 3,
+        out_specs=(anywhere, anywhere, anywhere, vmem),
+        scratch_shapes=[
+            pltpu.VMEM((3, 2 * n, cols, LANES), f32),
+            pltpu.VMEM((tiles, cols, LANES), bf),
+            pltpu.VMEM((tiles, cols, LANES), bf),
+            pltpu.VMEM((tiles, cols, LANES), bf),
+            pltpu.VMEM((tp, tok_rows, d), bf),
+            pltpu.VMEM((rows, cols), f32),
+            pltpu.VMEM((rows, cols), f32),
+            pltpu.VMEM((rows, cols), bf),
+            pltpu.VMEM((tiles, rows, LANES), bf),
+            pltpu.VMEM((tp, tiles, tok_rows, LANES), bf),
+            pltpu.VMEM((tok_rows, d), f32),
+            dma((3 * tiles,)), dma((3 * tiles,)), dma((3 * tiles,)), dma((3 * tiles,)),
+            dma((tp - 1,)), dma((tp,)),
+            dma((tp - 1, tiles)), dma((tp, tiles)), dma((3, tiles)), dma((3, 2 * n)),
+        ],
+        compiler_params=pltpu.CompilerParams(
+            collective_id=0, has_side_effects=True, vmem_limit_bytes=60 * 2**20
+        ),
+    )(
+        tokens, gate_master.T, up_master.T, down_master.T, norm_gain[None, :],
+        post_gain[None, :], post_bias[None, :],
+    )
+    return gate.T, up.T, down.T, result
+
+
 def solution(mesh):
+    grp, fs, tp = mesh.shape["grp"], mesh.shape["fs"], mesh.shape["tp"]
+
+    def local(tokens, gate_master, *rest):
+        rc, cols = gate_master.shape
+        n = rc // (2 * LANES)
+        fits = grp == 2 and fs > 1 and rc % (2 * LANES) == 0 and 2 * n * fs <= 32
+        fits = fits and cols % 16 == 0 and tokens.shape[0] % 16 == 0
+        if fits:
+            return fused(fs, tp, n, tokens, gate_master, *rest)
+        return plain(tokens, gate_master, *rest)
+
     return jax.shard_map(
         local,
         mesh=mesh,

time: 257 us -> 107 us (0.42)
  waiting for transfers between devices: 213 us -> 0 us
  Pallas kernels: 0 us -> 97.6 us
  between operations: 13.9 us -> 0.65 us
  other arithmetic: 11.4 us -> 0 us
  matrix products: 9.93 us -> 0 us
    all_gather x4 -> x0, waiting for transfers between devices: 188 us -> none  [the longest x1 60.2 us: local(): lax.all_gather(gate_piece, 'fs', axis=0, tiled=True)]
    pallas_call x0 -> x1, Pallas kernels: none -> 97.6 us  [fused(): pl.pallas_call(functools.partial(fused_kernel, fs, tp, n), out_shape=(rea...]
    reduce_scatter x1 -> x0, waiting for transfers between devices: 23.7 us -> none  [local(): lax.psum_scatter(lax.dot_general(hidden, down_ready, (((1,), (1,)), ((),...]
    dot_general x2 -> x0, matrix products: 9.93 us -> none  [the longest x1 6.89 us: local(): lax.dot_general(hidden, down_ready, (((1,), (1,)), ((), ())), preferred_e...]
    convert_element_type x4 -> x0, other arithmetic: 7.9 us -> none  [the longest x1 3.34 us: local(): up_piece = (gain_rows[:, None] * up_master).astype(jnp.bfloat16)]
    reduce_sum x3 -> x0, other arithmetic: 3.45 us -> none  [the longest x1 1.19 us: finish(): spread = jnp.mean(jnp.square(mixed - center), axis=-1, keepdims=True)]
    unnamed x19 -> x10, local copies, waits for them, and re-layouts: 7.21 us -> 8.94 us
  transfers between devices with their start and end apart: 5 -> 0, of which waited for: 5 -> 0; matrix products, arithmetic and copies ran while one was open for 3% -> 0% of each run, Pallas kernels for 0% -> 0%
where the time goes in v2:
time: 107 us
  Pallas kernels  97.6 us (91%)
  local copies, waits for them, and re-layouts  8.94 us (8%)
    pallas_call x1, Pallas kernels, fused(): pl.pallas_call(functools.partial(fused_kernel, fs, tp, n), out_shape=(rea...  97.6 us
    unnamed x10, local copies, waits for them, and re-layouts  8.94 us

profile of v2, /device:TPU:0, one launch (start us, length us, event | category | flops | bytes accessed | tf_op | source)
XLA Modules:
  0.0 107.2 jit_solution(383854526285588487)
XLA Ops:
  0.6 97.6 %shard_map.102 = (bf16[688,2048]{1,0:T(8,128)(2,1)}, bf16[688,2048]{1,0:T(8,128)(2,1)}, bf16[688,2048]{1,0:T(8,128)(2,1)}, bf16[64,2048]{1,0:T(8,128)(2,1)}) custom-call(bf16[64,2048]{1,0:T(8,128)(2,1)} %tok_ref.1, f32[688,512]{1,0:T(8,128)} %bitcast.12, f32[688,512]{1,0:T(8,128)} %bitcast.13, f32[688,512]{1,0:T(8,128)} %bitcast.14, f32[1,2048]{1,0:T(1,128)} %bitcast.15, ...), custom_call_target="tpu_custom_call" | custom-call | tf_op jit(solution)/shard_map/pallas_call | solution.py:314
  98.3 0.0 copy-start.1
  98.3 3.9 %copy.15 = bf16[2048,688]{0,1:T(8,128)(2,1)} copy(bf16[2048,688]{0,1:T(8,128)(2,1)} %bitcast.11) | data formatting | bytes 5636096
  102.1 0.0 copy-done.1
  102.1 0.0 copy-start
  102.1 1.6 %copy.16 = bf16[2048,688]{0,1:T(8,128)(2,1)} copy(bf16[2048,688]{0,1:T(8,128)(2,1)S(1)} %bitcast.10) | data formatting | bytes 5636096
  103.7 1.3 %copy-done = bf16[688,2048]{1,0:T(8,128)(2,1)S(1)} copy-done((bf16[688,2048]{1,0:T(8,128)(2,1)S(1)}, bf16[688,2048]{1,0:T(8,128)(2,1)}, u32[]{:S(2)}) %copy-start) | copy-done | bytes 2818072
  104.9 0.0 copy-start.2
  104.9 1.6 %copy.17 = bf16[2048,688]{0,1:T(8,128)(2,1)} copy(bf16[2048,688]{0,1:T(8,128)(2,1)S(1)} %bitcast.9) | data formatting | bytes 5636096
  106.5 0.0 copy-done.2
  106.5 0.7 copy.18
Async XLA Ops:
  98.3 3.9 %copy-start.1 = (bf16[688,2048]{1,0:T(8,128)(2,1)S(1)}, bf16[688,2048]{1,0:T(8,128)(2,1)}, u32[]{:S(2)}) copy-start(bf16[688,2048]{1,0:T(8,128)(2,1)} %get-tuple-element.9) | copy-start | bytes 8454148
  102.1 2.8 %copy-start = (bf16[688,2048]{1,0:T(8,128)(2,1)S(1)}, bf16[688,2048]{1,0:T(8,128)(2,1)}, u32[]{:S(2)}) copy-start(bf16[688,2048]{1,0:T(8,128)(2,1)} %get-tuple-element.10) | copy-start | bytes 8454148
  104.9 1.6 %copy-start.2 = (bf16[64,2048]{1,0:T(8,128)(2,1)S(1)}, bf16[64,2048]{1,0:T(8,128)(2,1)}, u32[]{:S(2)}) copy-start(bf16[64,2048]{1,0:T(8,128)(2,1)} %get-tuple-element.19) | copy-start | bytes 786436

commit v3 on v2

--- a/solution.py
+++ b/solution.py
@@ -232,7 +232,7 @@
         for m, c in first:
             arrived(m, c, p)
             waiting.append((m, c, p))
-            if len(waiting) > 1:
+            if len(waiting) > 2 * len(first):
                 crossed(*waiting.pop(0))
             if p > 0:
                 work(sums, 4)
@@ -250,10 +250,12 @@
         for m, c in second:
             arrived(m, c, p)
             waiting.append((m, c, p))
-            if len(waiting) > 1:
+            if p > 0 and len(waiting) > 2:
                 crossed(*waiting.pop(0))
             work(downs if p > 0 else sums, 4)
         if p == 0:
+            while waiting[0][0] < 2:
+                crossed(*waiting.pop(0))
             work(sums, len(sums))
             hid[...] = (jax.nn.silu(acc_g[...]) * acc_u[...]).astype(jnp.bfloat16)
             downs[:0] = [

time: 107 us -> 99.6 us (0.931)
  Pallas kernels: 97.6 us -> 89.8 us
    pallas_call x1, Pallas kernels: 97.6 us -> 89.8 us  [fused(): pl.pallas_call(functools.partial(fused_kernel, fs, tp, n), out_shape=(rea...]
where the time goes in v3:
time: 99.6 us; the launch traced here: 99.4 us
  Pallas kernels  89.8 us (90%)
  local copies, waits for them, and re-layouts  8.94 us (9%)
    pallas_call x1, Pallas kernels, fused(): pl.pallas_call(functools.partial(fused_kernel, fs, tp, n), out_shape=(rea...  89.8 us
    unnamed x10, local copies, waits for them, and re-layouts  8.94 us

profile of v3, /device:TPU:0, one launch (start us, length us, event | category | flops | bytes accessed | tf_op | source)
XLA Modules:
  0.0 99.4 jit_solution(16190318883525150280)
XLA Ops:
  0.6 89.8 %shard_map.102 = (bf16[688,2048]{1,0:T(8,128)(2,1)}, bf16[688,2048]{1,0:T(8,128)(2,1)}, bf16[688,2048]{1,0:T(8,128)(2,1)}, bf16[64,2048]{1,0:T(8,128)(2,1)}) custom-call(bf16[64,2048]{1,0:T(8,128)(2,1)} %tok_ref.1, f32[688,512]{1,0:T(8,128)} %bitcast.12, f32[688,512]{1,0:T(8,128)} %bitcast.13, f32[688,512]{1,0:T(8,128)} %bitcast.14, f32[1,2048]{1,0:T(1,128)} %bitcast.15, ...), custom_call_target="tpu_custom_call" | custom-call | tf_op jit(solution)/shard_map/pallas_call | solution.py:316
  90.5 0.0 copy-start.1
  90.5 3.9 %copy.15 = bf16[2048,688]{0,1:T(8,128)(2,1)} copy(bf16[2048,688]{0,1:T(8,128)(2,1)} %bitcast.11) | data formatting | bytes 5636096
  94.3 0.0 copy-done.1
  94.3 0.0 copy-start
  94.3 1.6 %copy.16 = bf16[2048,688]{0,1:T(8,128)(2,1)} copy(bf16[2048,688]{0,1:T(8,128)(2,1)S(1)} %bitcast.10) | data formatting | bytes 5636096
  95.9 1.3 %copy-done = bf16[688,2048]{1,0:T(8,128)(2,1)S(1)} copy-done((bf16[688,2048]{1,0:T(8,128)(2,1)S(1)}, bf16[688,2048]{1,0:T(8,128)(2,1)}, u32[]{:S(2)}) %copy-start) | copy-done | bytes 2818072
  97.2 0.0 copy-start.2
  97.2 1.6 %copy.17 = bf16[2048,688]{0,1:T(8,128)(2,1)} copy(bf16[2048,688]{0,1:T(8,128)(2,1)S(1)} %bitcast.9) | data formatting | bytes 5636096
  98.7 0.0 copy-done.2
  98.7 0.7 copy.18
Async XLA Ops:
  90.5 3.9 %copy-start.1 = (bf16[688,2048]{1,0:T(8,128)(2,1)S(1)}, bf16[688,2048]{1,0:T(8,128)(2,1)}, u32[]{:S(2)}) copy-start(bf16[688,2048]{1,0:T(8,128)(2,1)} %get-tuple-element.9) | copy-start | bytes 8454148
  94.3 2.8 %copy-start = (bf16[688,2048]{1,0:T(8,128)(2,1)S(1)}, bf16[688,2048]{1,0:T(8,128)(2,1)}, u32[]{:S(2)}) copy-start(bf16[688,2048]{1,0:T(8,128)(2,1)} %get-tuple-element.10) | copy-start | bytes 8454148
  97.2 1.6 %copy-start.2 = (bf16[64,2048]{1,0:T(8,128)(2,1)S(1)}, bf16[64,2048]{1,0:T(8,128)(2,1)}, u32[]{:S(2)}) copy-start(bf16[64,2048]{1,0:T(8,128)(2,1)} %get-tuple-element.19) | copy-start | bytes 786436
